TPU v7x, 32 devices: a whole 2x2x4 slice. The times are simulated.
32 devices in a mesh: sp: 8 (over z, core), tp: 4 (over y, x).
Axes of the slice: x: 2, y: 2, z: 4, core: 2. Of those that a mesh axis runs over, the one named last changes fastest.
Arguments:
- tokens: bfloat16 [2, 6144, 4096], P(None, 'sp', 'tp'), may hold values from -6 to 6
- w_key: bfloat16 [4096, 2048], P(None, 'tp'), may hold values from -0.09375 to 0.09375
- w_value: bfloat16 [4096, 2048], P(None, 'tp'), may hold values from -0.09375 to 0.09375
- w_gate: bfloat16 [4096, 4, 16], replicated, may hold values from -0.09375 to 0.09375
- forget_bias: float32 [2, 16], replicated, may hold values from 3.9 to 13, as said below
- log_shift: float32 [2, 4, 16, 6144], P(None, None, 'tp', 'sp'), may hold values from -5 to 121, as said below
- new_query: bfloat16 [2, 1024, 2048], P(None, 'sp', 'tp'), may hold values from -6 to 6
Outputs:
- cache_matrix: bfloat16 [2, 2, 16, 128, 128], P(None, None, 'tp')
- cache_norm: float32 [2, 2, 16, 128], P(None, None, 'tp')
- cache_max: float32 [2, 2, 16], P(None, None, 'tp')
- first_read: bfloat16 [2, 1024, 2048], P(None, 'sp', 'tp')
Inputs may be any that keep to these rules, and one draw needn't show every extreme that they name: `forget_bias`: added to the forget gates' pre-activations, by direction and head. `log_shift`: rows 0 and 2 are added to the input gates of the two directions; rows 1 and 3 are added to the log forget gates and are never positive.
All inputs are finite; a program needn't handle non-finite values.
Results may differ from a plain program's by a relative error of at most 0.024.
Values may be sent and summed in bfloat16 or wider, within the bound.
No kernel may reach another device: no remote copies, remote signals or barrier semaphores. Data moves between devices by JAX's collectives and lax.ppermute only.
A program may use at most 64 MiB of HBM per device.

v0:
```python
import jax
import jax.numpy as jnp
from jax import lax
from jax.sharding import PartitionSpec as P

HEAD = 128


def combined_all(array, axis, combine):
    everything = jax.tree.map(lambda part: lax.all_gather(part, axis), array)
    leading = jax.tree.map(lambda part: part[0], everything)

    def lap(k, so_far):
        return combine(so_far, jax.tree.map(lambda part: part[k], everything))

    return lax.fori_loop(1, lax.axis_size(axis), lap, leading)


def joint_max(earlier, latter):
    memory_a, norm_a, high_a = earlier
    memory_b, norm_b, high_b = latter
    highest = jnp.maximum(high_a, high_b)
    carried = jnp.exp(high_a - highest)
    own_part = jnp.exp(high_b - highest)
    memory = memory_a * carried[..., None, None] + memory_b * own_part[..., None, None]
    norm_sum = norm_a * carried[..., None] + norm_b * own_part[..., None]
    return (memory, norm_sum, highest)


def on_device(tokens, w_key, w_value, w_gate, forget_bias, log_shift, new_query):
    seq_count, seg_len, part_width = tokens.shape
    per_head = w_key.shape[1] // HEAD
    row_count = seq_count * seg_len
    first_head = lax.axis_index("tp") * per_head
    gate_cols = lax.dynamic_slice_in_dim(w_gate, first_head, per_head, 2).reshape(
        w_gate.shape[0], 4 * per_head
    )
    bias_own = lax.dynamic_slice_in_dim(forget_bias, first_head, per_head, 1)
    piece = lax.all_gather(tokens, "tp", axis=2, tiled=True)
    piece_width = piece.shape[2]
    flat_piece = piece.reshape(row_count, piece_width)
    key_sum = jnp.dot(flat_piece, w_key, preferred_element_type=jnp.float32)
    value_sum = jnp.dot(flat_piece, w_value, preferred_element_type=jnp.float32)
    gate_sum = jnp.dot(flat_piece, gate_cols, preferred_element_type=jnp.float32)
    key_rows = key_sum.astype(jnp.bfloat16).reshape(seq_count, seg_len, per_head, HEAD)
    value_rows = value_sum.astype(jnp.bfloat16).reshape(seq_count, seg_len, per_head, HEAD)
    gates = gate_sum.reshape(seq_count, seg_len, 4, per_head).transpose(0, 2, 3, 1)
    input_fwd = gates[:, 0] + log_shift[:, 0]
    forget_fwd = jax.nn.log_sigmoid(gates[:, 1] + bias_own[0][None, :, None]) + log_shift[:, 1]
    input_bwd = gates[:, 2] + log_shift[:, 2]
    forget_bwd = jax.nn.log_sigmoid(gates[:, 3] + bias_own[1][None, :, None]) + log_shift[:, 3]
    climb_fwd = jnp.cumsum(forget_fwd, axis=-1)
    total_fwd = climb_fwd[..., -1]
    weight_fwd = total_fwd[..., None] - climb_fwd + input_fwd
    climb_bwd = jnp.cumsum(forget_bwd, axis=-1)
    total_bwd = climb_bwd[..., -1]
    weight_bwd = climb_bwd - forget_bwd + input_bwd
    weights = jnp.stack([weight_fwd, weight_bwd], axis=1)
    totals = jnp.stack([total_fwd, total_bwd], axis=1)
    local_top = jnp.max(weights, axis=-1)
    scale_now = jnp.exp(weights - local_top[..., None])
    key_f = key_rows.astype(jnp.float32).transpose(0, 2, 1, 3) * HEAD ** (-0.5)
    value_f = value_rows.astype(jnp.float32).transpose(0, 2, 1, 3)
    weighted = scale_now[..., None] * key_f[:, None]
    memory = jnp.einsum("bjhld,bhle->bjhde", weighted, value_f, precision=lax.Precision.HIGHEST)
    norm_sum = jnp.sum(weighted, axis=3)
    every_total = lax.all_gather(totals[None], "sp", axis=0, tiled=True)
    my_index = lax.axis_index("sp")
    sources = jnp.arange(every_total.shape[0])[:, None, None, None]
    direction = jnp.arange(2)[None, None, :, None]
    counted = jnp.where(direction == 0, sources > my_index, sources < my_index)
    passed = jnp.sum(jnp.where(counted, every_total, 0.0), axis=0)
    total_all = jnp.sum(every_total, axis=0)
    memory_all, norm_all, top_all = combined_all(
        (memory, norm_sum, local_top + passed), "sp", joint_max
    )
    cache_max = jnp.maximum(total_all, top_all)
    rescale = jnp.exp(top_all - cache_max)
    cache_matrix = (memory_all * rescale[..., None, None]).astype(jnp.bfloat16)
    cache_norm = norm_all * rescale[..., None]
    new_count = new_query.shape[1]
    queries = new_query.reshape(seq_count, new_count, per_head, HEAD)
    numerator = jnp.einsum(
        "bthd,bjhde->bjthe", queries, cache_matrix, preferred_element_type=jnp.float32
    )
    denominator = jnp.einsum(
        "bthd,bjhd->bjth", queries.astype(jnp.float32), cache_norm, precision=lax.Precision.HIGHEST
    )
    divisor = jnp.maximum(jnp.abs(denominator), 1.0)
    first_read = jnp.sum(numerator / divisor[..., None], axis=1)
    first_read = first_read.reshape(seq_count, new_count, per_head * HEAD).astype(jnp.bfloat16)
    return (cache_matrix, cache_norm, cache_max, first_read)


def solution(mesh):
    return jax.shard_map(
        on_device,
        mesh=mesh,
        in_specs=(
            P(None, "sp", "tp"),
            P(None, "tp"),
            P(None, "tp"),
            P(),
            P(),
            P(None, None, "tp", "sp"),
            P(None, "sp", "tp"),
        ),
        out_specs=(
            P(None, None, "tp", None, None),
            P(None, None, "tp", None),
            P(None, None, "tp"),
            P(None, "sp", "tp"),
        ),
        check_vma=False,
    )
```

profile of v0, /device:TPU:0, one launch (start us, length us, event | category | flops | bytes accessed | tf_op | source)
XLA Modules:
  0.0 296.8 jit_solution(11978005785362571793)
XLA Ops:
  7.2 0.0 copy-start
  7.2 0.0 all-gather.7.cloned.1.call-start
  7.2 0.7 all-gather.7.cloned.1.call-update
  7.9 0.0 all-gather.9.cloned.1.call-start
  8.0 0.8 fusion.34
  8.8 0.1 constant_dynamic-slice_fusion.1
  8.9 0.8 constant_dynamic-slice_fusion
  9.7 125.3 %all-gather.7.cloned.1.call-done = bf16[2,768,4096]{2,1,0:T(8,128)(2,1)} async-done(((bf16[2,768,1024]{2,1,0:T(8,128)(2,1)}), bf16[2,768,4096]{2,1,0:T(8,128)(2,1)}) %all-gather.7.cloned.1.call-update) | async-done | bytes 12582928 | tf_op jit(solution)/shard_map/all_gather | solution.py:39
  135.0 7.9 %convolution_bitcast_fusion = f32[1536,16]{0,1:T(8,128)S(1)} fusion(bf16[4096,16]{0,1:T(8,128)(2,1)S(1)} %reshape.198, bf16[1536,4096]{1,0:T(8,128)(2,1)} %bitcast.91), kind=kOutput, calls=%fused_computation.16 | convolution fusion | flops 201326592 | bytes 12812288 | tf_op jit(solution)/shard_map/dot_general | solution.py:44
  142.9 0.1 reshape.199
  143.1 0.1 fusion.22
  143.2 2.3 reduce-window.14
  145.5 0.2 slice_reduce_fusion.1
  145.7 0.4 reduce-window.15
  146.0 0.1 broadcast_add_fusion.1
  146.2 0.2 slice_reduce_fusion.3
  146.3 2.3 reduce-window.16
  148.6 0.2 slice_reduce_fusion
  148.7 0.4 reduce-window.19
  149.1 0.1 broadcast_add_fusion
  149.2 0.1 fusion.30
  149.3 0.1 fusion.25
  149.4 0.1 subtract_exponential_fusion.1
  149.6 11.9 %convolution_convert_fusion.1 = bf16[1536,512]{1,0:T(8,128)(2,1)} fusion(bf16[1536,4096]{1,0:T(8,128)(2,1)} %bitcast.92, bf16[4096,512]{1,0:T(8,128)(2,1)} %param.11), kind=kOutput, calls=%fused_computation.15 | convolution fusion | flops 6443237376 | bytes 18350080 | tf_op jit(solution)/shard_map/dot_general | solution.py:43
  161.5 10.8 %convert_multiply_fusion = f32[1536,512]{1,0:T(8,128)} fusion(bf16[1536,4096]{1,0:T(8,128)(2,1)} %bitcast.93, bf16[4096,512]{1,0:T(8,128)(2,1)S(1)} %copy-done.5), kind=kOutput, calls=%fused_computation.12 | convolution fusion | flops 6444810240 | bytes 19922944 | tf_op jit(solution)/shard_map/dot_general | solution.py:42
  172.2 4.9 %mul.152 = f32[2,768,4,128]{3,2,1,0:T(4,128)} reshape(f32[1536,512]{1,0:T(8,128)} %convert_multiply_fusion) | data formatting | bytes 6291456 | tf_op jit(solution)/shard_map/mul | solution.py:62
  177.1 3.8 %copy.65 = f32[2,4,768,128]{3,2,1,0:T(8,128)} copy(f32[2,4,768,128]{3,1,2,0:T(4,128)} %bitcast.94) | data formatting | bytes 6291456 | tf_op jit(solution)/shard_map/mul | solution.py:62
  180.9 2.4 reshape.197
  183.3 2.3 copy.59
  185.6 5.3 %fusion.8 = f32[2,2,4,128,128]{3,4,1,2,0:T(8,128)S(1)} fusion(f32[2,4,768,128]{3,2,1,0:T(8,128)} %copy.65, f32[2,2,4,768]{3,1,2,0:T(2,128)S(1)} %copy.64, bf16[2,768,4,128]{1,3,2,0:T(8,128)(2,1)} %copy.59), kind=kOutput, calls=%fused_computation.18 | convolution fusion | flops 2417491968 | bytes 5816320 | tf_op jit(solution)/shard_map/bjhld,bhle->bjhde/dot_general | solution.py:65
  190.9 1.3 copy.66
  192.2 0.0 all-gather.9.cloned.1.call-update
  192.2 0.1 reshape.202
  192.3 0.1 broadcast_select_fusion
  192.4 0.2 slice_reduce_fusion.2
  192.6 12.8 %all-gather.2 = f32[16,2,4]{2,1,0:T(2,128)S(1)} all-gather(f32[2,2,4]{2,1,0:T(2,128)S(1)} %copy.68), channel_id=4, replica_groups=mesh['sp'=8,'tp'=4] {'sp'}, dimensions={0}, use_global_device_ids=true | all-gather | bytes 576 | tf_op jit(solution)/shard_map/all_gather | solution.py:67
  205.4 0.1 fusion.32
  205.5 14.4 %all-gather.3 = f32[16,2,4]{2,1,0:T(2,128)S(1)} all-gather(f32[2,2,4]{2,1,0:T(2,128)S(1)} %copy.70), channel_id=5, replica_groups=mesh['sp'=8,'tp'=4] {'sp'}, dimensions={0}, use_global_device_ids=true | all-gather | bytes 576 | tf_op jit(solution)/shard_map/all_gather | solution.py:10
  219.9 3.8 %multiply_reduce_fusion = f32[2,2,4,128]{3,1,2,0:T(2,128)S(1)} fusion(f32[2,4,768,128]{3,2,1,0:T(8,128)} %copy.65, f32[2,2,4,768]{3,1,2,0:T(2,128)S(1)} %copy.64), kind=kLoop, calls=%fused_computation.8 | loop fusion | flops 3143680 | bytes 3203072 | tf_op jit(solution)/shard_map/reduce_sum | solution.py:66
  223.7 14.5 %all-gather.1 = f32[16,2,4,128]{3,2,1,0:T(4,128)S(1)} all-gather(f32[2,2,4,128]{3,2,1,0:T(4,128)S(1)} %copy.67), channel_id=3, replica_groups=mesh['sp'=8,'tp'=4] {'sp'}, dimensions={0}, use_global_device_ids=true | all-gather | bytes 73728 | tf_op jit(solution)/shard_map/all_gather | solution.py:10
  238.3 36.6 %all-gather.9.cloned.1.call-done = f32[16,2,4,128,128]{4,3,2,1,0:T(8,128)} async-done(((f32[2,2,4,128,128]{4,3,2,1,0:T(8,128)}), f32[16,2,4,128,128]{4,3,2,1,0:T(8,128)}) %all-gather.9.cloned.1.call-update) | async-done | bytes 8388624 | tf_op jit(solution)/shard_map/all_gather | solution.py:10
  274.9 1.3 slice.88
  276.2 11.2 %while.19 = (s32[]{:T(128)}, f32[2,2,4,128,128]{4,3,2,1,0:T(8,128)S(1)}, f32[2,2,4,128]{3,2,1,0:T(4,128)S(1)}, f32[2,2,4]{2,1,0:T(2,128)S(1)}, f32[8,2,2,4]{3,2,...) while((s32[]{:T(128)}, ...), condition=%wide.region_8.9_spmd, body=%wide.region_7.8_spmd.sunk | while | flops 792629 | bytes 3171159 | solution.py:16
  276.3 0.1 fusion.47
  276.4 1.4 fusion.46
  277.9 0.1 fusion.47
  278.0 1.4 fusion.46
  279.5 0.1 fusion.47
  279.6 1.4 fusion.46
  281.1 0.1 fusion.47
  281.2 1.4 fusion.46
  282.7 0.1 fusion.47
  282.8 1.4 fusion.46
  284.3 0.1 fusion.47
  284.4 1.4 fusion.46
  285.9 0.1 fusion.47
  286.0 1.4 fusion.46
  287.4 0.6 copy.81
  288.0 0.2 multiply_convert_fusion
  288.2 0.0 copy-start.2
  288.2 0.1 broadcast_multiply_fusion
  288.3 0.5 fusion.16
  288.8 0.4 fusion.14
  289.1 0.9 copy.82
  (49 shorter events, 0.5 us)
Async XLA Ops:
  7.2 1.6 copy-start
  7.2 127.8 %all-gather.7.cloned.1.call-start = ((), (), s32[]{:S(2)}) async-start(), calls=%async_computation | async-start | bytes 15728640 | tf_op jit(solution)/shard_map/all_gather | solution.py:39
  7.9 267.0 %all-gather.9.cloned.1.call-start = ((), (), s32[]{:S(2)}) async-start(), calls=%async_computation.1 | async-start | bytes 9437184 | tf_op jit(solution)/shard_map/all_gather | solution.py:10
  135.0 14.2 %copy-start.3 = (f32[2,4,4,768]{3,2,1,0:T(4,128)S(1)}, f32[2,4,4,768]{3,2,1,0:T(4,128)}, u32[]{:S(2)}) copy-start(f32[2,4,4,768]{3,2,1,0:T(4,128)} %param.14) | copy-start | bytes 294916
  149.6 11.9 %copy-start.5 = (bf16[4096,512]{1,0:T(8,128)(2,1)S(1)}, bf16[4096,512]{1,0:T(8,128)(2,1)}, u32[]{:S(2)}) copy-start(bf16[4096,512]{1,0:T(8,128)(2,1)} %param.10) | copy-start | bytes 12582916
  185.6 6.7 %copy-start.1 = (bf16[2,128,512]{2,1,0:T(8,128)(2,1)S(1)}, bf16[2,128,512]{2,1,0:T(8,128)(2,1)}, u32[]{:S(2)}) copy-start(bf16[2,128,512]{2,1,0:T(8,128)(2,1)} %param.15) | copy-start | bytes 786436
  288.2 1.8 copy-start.2
  288.3 1.7 copy-start.4
Sparse Core Ops, SparseCore 0:
  9.8 125.0 all-gather.6
  192.3 82.5 all-gather.8
where the time goes:
time: 298 us; the launch traced here: 297 us
  waiting for transfers between devices  163 us (55%)
  blocking collectives  41.7 us (14%)
  matrix products  36.8 us (12%)
  other arithmetic  21 us (7%)
  local copies, waits for them, and re-layouts  20 us (7%)
  between operations  14.3 us (5%)
    all_gather x1, waiting for transfers between devices, on_device(): piece = lax.all_gather(tokens, 'tp', axis=2, tiled=True)  125 us
    all_gather x1, waiting for transfers between devices, combined_all(): everything = jax.tree.map(lambda part: lax.all_gather(part, axis), array)  36.6 us
    all_gather x2, blocking collectives, combined_all(): everything = jax.tree.map(lambda part: lax.all_gather(part, axis), array)  28.9 us
    all_gather x1, blocking collectives, on_device(): every_total = lax.all_gather(totals[None], 'sp', axis=0, tiled=True)  12.8 us
    dot_general x1, matrix products, on_device(): value_sum = jnp.dot(flat_piece, w_value, preferred_element_type=jnp.float32)  11.9 us
    dot_general x1, matrix products, on_device(): key_sum = jnp.dot(flat_piece, w_key, preferred_element_type=jnp.float32)  10.8 us
    add x7, other arithmetic, joint_max(): memory_a * carried[..., None, None] + memory_b * own_part[..., None, None]  10.1 us
    mul x2, local copies, waits for them, and re-layouts, on_device(): key_f = key_rows.astype(jnp.float32).transpose(0, 2, 1, 3) * HEAD ** (-0.5)  8.72 us
  transfers between devices with their start and end apart: 2, of which 2 were waited for; matrix products, arithmetic and copies ran while one was open for 2% of the time, Pallas kernels for 0%

commit v1 on v0

--- a/solution.py
+++ b/solution.py
@@ -36,7 +36,8 @@
         w_gate.shape[0], 4 * per_head
     )
     bias_own = lax.dynamic_slice_in_dim(forget_bias, first_head, per_head, 1)
-    piece = lax.all_gather(tokens, "tp", axis=2, tiled=True)
+    shards = lax.all_gather(tokens, "tp", axis=0, tiled=False)
+    piece = jnp.concatenate(shards, axis=2)
     piece_width = piece.shape[2]
     flat_piece = piece.reshape(row_count, piece_width)
     key_sum = jnp.dot(flat_piece, w_key, preferred_element_type=jnp.float32)

time: 298 us -> 320 us (1.074)
  local copies, waits for them, and re-layouts: 20 us -> 45.8 us
  matrix products: 36.8 us -> 33.3 us
    all_gather x0 -> x1, local copies, waits for them, and re-layouts: none -> 16.2 us  [on_device(): shards = lax.all_gather(tokens, 'tp', axis=0, tiled=False)]
    unnamed x14 -> x17, local copies, waits for them, and re-layouts: 1.46 us -> 11 us
    dot_general x1, matrix products: 7.95 us -> 3.34 us  [on_device(): jnp.dot(flat_piece, gate_cols, preferred_element_type=jnp.float32)]
where the time goes in v1:
time: 320 us; the launch traced here: 319 us
  waiting for transfers between devices  161 us (50%)
  local copies, waits for them, and re-layouts  45.8 us (14%)
  blocking collectives  42.8 us (13%)
  matrix products  33.3 us (10%)
  other arithmetic  21 us (7%)
  between operations  14.3 us (4%)
    all_gather x1, waiting for transfers between devices, on_device(): shards = lax.all_gather(tokens, 'tp', axis=0, tiled=False)  125 us
    all_gather x1, waiting for transfers between devices, combined_all(): everything = jax.tree.map(lambda part: lax.all_gather(part, axis), array)  35.5 us
    all_gather x2, blocking collectives, combined_all(): everything = jax.tree.map(lambda part: lax.all_gather(part, axis), array)  27.9 us
    all_gather x1, local copies, waits for them, and re-layouts, on_device(): shards = lax.all_gather(tokens, 'tp', axis=0, tiled=False)  16.2 us
    all_gather x1, blocking collectives, on_device(): every_total = lax.all_gather(totals[None], 'sp', axis=0, tiled=True)  14.9 us
    dot_general x1, matrix products, on_device(): key_sum = jnp.dot(flat_piece, w_key, preferred_element_type=jnp.float32)  12 us
    dot_general x1, matrix products, on_device(): value_sum = jnp.dot(flat_piece, w_value, preferred_element_type=jnp.float32)  11.7 us
    unnamed x17, local copies, waits for them, and re-layouts  11 us
  transfers between devices with their start and end apart: 2, of which 2 were waited for; matrix products, arithmetic and copies ran while one was open for 2% of the time, Pallas kernels for 0%

profile of v1, /device:TPU:0, one launch (start us, length us, event | category | flops | bytes accessed | tf_op | source)
XLA Modules:
  0.0 318.8 jit_solution(14364375979871126477)
XLA Ops:
  7.2 0.7 all-gather.8.cloned.1.call-update
  7.9 0.0 all-gather.10.cloned.1.call-start
  8.0 0.2 copy-done
  8.2 0.1 constant_dynamic-slice_fusion.1
  8.3 0.8 fusion.34
  9.1 0.8 constant_dynamic-slice_fusion
  9.9 125.1 %all-gather.8.cloned.1.call-done = bf16[8,768,1024]{2,1,0:T(8,128)(2,1)} async-done(((bf16[2,768,1024]{2,1,0:T(8,128)(2,1)}), bf16[8,768,1024]{2,1,0:T(8,128)(2,1)}) %all-gather.8.cloned.1.call-update) | async-done | bytes 12582928 | tf_op jit(solution)/shard_map/all_gather | solution.py:39
  135.0 16.2 %copy.61 = bf16[4,2,768,1024]{3,0,2,1:T(4,128)(2,1)S(1)} copy(bf16[4,2,768,1024]{3,2,1,0:T(8,128)(2,1)} %bitcast.99) | data formatting | bytes 25165824 | tf_op jit(solution)/shard_map/all_gather | solution.py:39
  151.1 4.7 %copy.97 = bf16[192,8,4,1024]{3,1,2,0:T(8,128)(2,1)S(1)} copy(bf16[192,8,4,1024]{3,2,1,0:T(4,128)(2,1)S(1)} %bitcast.98) | data formatting | bytes 25165824
  155.8 4.6 %copy-done.2 = bf16[192,8,4,1024]{3,1,2,0:T(8,128)(2,1)} copy-done((bf16[192,8,4,1024]{3,1,2,0:T(8,128)(2,1)}, bf16[192,8,4,1024]{3,1,2,0:T(8,128)(2,1)S(1)}, u32[]{:S(2)}) %copy-start.2) | copy-done | bytes 12582936
  160.4 3.3 %convolution_bitcast_fusion = f32[1536,16]{0,1:T(8,128)S(1)} fusion(bf16[4096,16]{0,1:T(8,128)(2,1)S(1)} %reshape.198, bf16[1536,4096]{1,0:T(8,128)(2,1)S(1)} %bitcast.95), kind=kOutput, calls=%fused_computation.16 | convolution fusion | flops 201326592 | bytes 12812288 | tf_op jit(solution)/shard_map/dot_general | solution.py:45
  163.7 0.1 reshape.199
  163.9 0.1 fusion.22
  164.0 2.3 reduce-window.14
  166.3 0.2 slice_reduce_fusion.1
  166.5 0.4 reduce-window.15
  166.8 0.1 broadcast_add_fusion.1
  167.0 12.0 %convert_multiply_fusion = f32[1536,512]{1,0:T(8,128)} fusion(bf16[1536,4096]{1,0:T(8,128)(2,1)} %bitcast.96, bf16[4096,512]{1,0:T(8,128)(2,1)} %param.10), kind=kOutput, calls=%fused_computation.12 | convolution fusion | flops 6444810240 | bytes 19922944 | tf_op jit(solution)/shard_map/dot_general | solution.py:43
  179.0 4.9 %mul.152 = f32[2,768,4,128]{3,2,1,0:T(4,128)} reshape(f32[1536,512]{1,0:T(8,128)} %convert_multiply_fusion) | data formatting | bytes 6291456 | tf_op jit(solution)/shard_map/mul | solution.py:63
  183.9 3.8 %copy.68 = f32[2,4,768,128]{3,2,1,0:T(8,128)} copy(f32[2,4,768,128]{3,1,2,0:T(4,128)} %bitcast.100) | data formatting | bytes 6291456 | tf_op jit(solution)/shard_map/mul | solution.py:63
  187.7 0.2 slice_reduce_fusion.3
  187.8 2.3 reduce-window.16
  190.1 0.2 slice_reduce_fusion
  190.2 0.4 reduce-window.19
  190.6 0.1 broadcast_add_fusion
  190.7 0.1 fusion.30
  190.8 0.1 fusion.25
  190.9 0.1 subtract_exponential_fusion.1
  191.1 11.7 %convolution_convert_fusion.1 = bf16[1536,512]{1,0:T(8,128)(2,1)} fusion(bf16[1536,4096]{1,0:T(8,128)(2,1)} %bitcast.97, bf16[4096,512]{1,0:T(8,128)(2,1)} %param.11), kind=kOutput, calls=%fused_computation.15 | convolution fusion | flops 6443237376 | bytes 18350080 | tf_op jit(solution)/shard_map/dot_general | solution.py:44
  202.8 2.4 reshape.197
  205.2 2.3 copy.62
  207.5 5.3 %fusion.8 = f32[2,2,4,128,128]{3,4,1,2,0:T(8,128)S(1)} fusion(f32[2,4,768,128]{3,2,1,0:T(8,128)} %copy.68, f32[2,2,4,768]{3,1,2,0:T(2,128)S(1)} %copy.67, bf16[2,768,4,128]{1,3,2,0:T(8,128)(2,1)} %copy.62), kind=kOutput, calls=%fused_computation.18 | convolution fusion | flops 2417491968 | bytes 5816320 | tf_op jit(solution)/shard_map/bjhld,bhle->bjhde/dot_general | solution.py:66
  212.8 1.4 copy.69
  214.2 0.1 reshape.202
  214.3 0.1 broadcast_select_fusion
  214.4 3.8 %multiply_reduce_fusion = f32[2,2,4,128]{3,1,2,0:T(2,128)S(1)} fusion(f32[2,4,768,128]{3,2,1,0:T(8,128)} %copy.68, f32[2,2,4,768]{3,1,2,0:T(2,128)S(1)} %copy.67), kind=kLoop, calls=%fused_computation.8 | loop fusion | flops 3143680 | bytes 3203072 | tf_op jit(solution)/shard_map/reduce_sum | solution.py:67
  218.2 14.5 %all-gather.2 = f32[16,2,4,128]{3,2,1,0:T(4,128)S(1)} all-gather(f32[2,2,4,128]{3,2,1,0:T(4,128)S(1)} %copy.70), channel_id=4, replica_groups=mesh['sp'=8,'tp'=4] {'sp'}, dimensions={0}, use_global_device_ids=true | all-gather | bytes 73728 | tf_op jit(solution)/shard_map/all_gather | solution.py:10
  232.8 0.2 slice_reduce_fusion.2
  232.9 14.9 %all-gather.3 = f32[16,2,4]{2,1,0:T(2,128)S(1)} all-gather(f32[2,2,4]{2,1,0:T(2,128)S(1)} %copy.71), channel_id=5, replica_groups=mesh['sp'=8,'tp'=4] {'sp'}, dimensions={0}, use_global_device_ids=true | all-gather | bytes 576 | tf_op jit(solution)/shard_map/all_gather | solution.py:68
  247.8 0.1 fusion.32
  247.9 13.4 %all-gather.4 = f32[16,2,4]{2,1,0:T(2,128)S(1)} all-gather(f32[2,2,4]{2,1,0:T(2,128)S(1)} %copy.73), channel_id=6, replica_groups=mesh['sp'=8,'tp'=4] {'sp'}, dimensions={0}, use_global_device_ids=true | all-gather | bytes 576 | tf_op jit(solution)/shard_map/all_gather | solution.py:10
  261.4 35.5 %all-gather.10.cloned.1.call-done = f32[16,2,4,128,128]{4,3,2,1,0:T(8,128)} async-done(((f32[2,2,4,128,128]{4,3,2,1,0:T(8,128)}), f32[16,2,4,128,128]{4,3,2,1,0:T(8,128)}) %all-gather.10.cloned.1.call-update) | async-done | bytes 8388624 | tf_op jit(solution)/shard_map/all_gather | solution.py:10
  296.9 1.3 slice.88
  298.2 11.1 %while.19 = (s32[]{:T(128)}, f32[2,2,4,128,128]{4,3,2,1,0:T(8,128)S(1)}, f32[2,2,4,128]{3,2,1,0:T(4,128)S(1)}, f32[2,2,4]{2,1,0:T(2,128)S(1)}, f32[8,2,2,4]{3,2,...) while((s32[]{:T(128)}, ...), condition=%wide.region_8.9_spmd, body=%wide.region_7.8_spmd.sunk | while | flops 792629 | bytes 3171167 | solution.py:16
  298.2 1.4 fusion.46
  299.7 0.1 fusion.47
  299.8 1.4 fusion.46
  301.3 0.1 fusion.47
  301.4 1.4 fusion.46
  302.8 0.1 fusion.47
  303.0 1.4 fusion.46
  304.4 0.1 fusion.47
  304.5 1.4 fusion.46
  306.0 0.1 fusion.47
  306.1 1.4 fusion.46
  307.6 0.1 fusion.47
  307.7 1.4 fusion.46
  309.1 0.1 fusion.47
  309.3 0.2 multiply_convert_fusion
  309.4 0.1 broadcast_multiply_fusion
  309.5 0.7 copy.84
  310.2 0.5 fusion.16
  310.7 0.4 fusion.14
  311.1 0.9 copy.85
  (53 shorter events, 0.5 us)
Async XLA Ops:
  7.2 1.1 copy-start
  7.2 127.8 %all-gather.8.cloned.1.call-start = ((), (), s32[]{:S(2)}) async-start(), calls=%async_computation | async-start | bytes 15728640 | tf_op jit(solution)/shard_map/all_gather | solution.py:39
  7.9 289.0 %all-gather.10.cloned.1.call-start = ((), (), s32[]{:S(2)}) async-start(), calls=%async_computation.1 | async-start | bytes 9437184 | tf_op jit(solution)/shard_map/all_gather | solution.py:10
  155.8 4.6 %copy-start.2 = (bf16[192,8,4,1024]{3,1,2,0:T(8,128)(2,1)}, bf16[192,8,4,1024]{3,1,2,0:T(8,128)(2,1)S(1)}, u32[]{:S(2)}) copy-start(bf16[192,8,4,1024]{3,1,2,0:T(8,128)(2,1)S(1)} %copy.97) | copy-start | bytes 37748740
  183.9 6.8 %copy-start.5 = (f32[2,4,4,768]{3,2,1,0:T(4,128)S(1)}, f32[2,4,4,768]{3,2,1,0:T(4,128)}, u32[]{:S(2)}) copy-start(f32[2,4,4,768]{3,2,1,0:T(4,128)} %param.14) | copy-start | bytes 294916
  207.5 6.8 %copy-start.3 = (bf16[2,128,512]{2,1,0:T(8,128)(2,1)S(1)}, bf16[2,128,512]{2,1,0:T(8,128)(2,1)}, u32[]{:S(2)}) copy-start(bf16[2,128,512]{2,1,0:T(8,128)(2,1)} %param.15) | copy-start | bytes 786436
  309.2 2.7 copy-start.1
  309.4 2.5 copy-start.4
  309.5 2.4 copy-start.6
Sparse Core Ops, SparseCore 0:
  9.8 125.0 all-gather.7
  214.3 82.5 all-gather.9
